TPU v7x, 32 devices: a whole 2x2x4 slice. The times are simulated.
32 devices in a mesh: kv: 16 (over z, y, core), tp: 2 (over x).
Axes of the slice: x: 2, y: 2, z: 4, core: 2. Of those that a mesh axis runs over, the one named last changes fastest.
Arguments:
- tokens: bfloat16 [12, 2048], replicated, may hold values from -6 to 6
- w_query: bfloat16 [2048, 2048], P(None, 'tp'), may hold values from -0.125 to 0.125
- w_key: bfloat16 [2048, 512], P(None, 'tp'), may hold values from -0.125 to 0.125
- w_value: bfloat16 [2048, 512], P(None, 'tp'), may hold values from -0.125 to 0.125
- w_gate: bfloat16 [2048, 32], replicated, may hold values from -0.125 to 0.125
- w_out: bfloat16 [2048, 2048], P(None, 'tp'), may hold values from -0.125 to 0.125
- key_cache: bfloat16 [12, 4096, 512], P(None, 'kv', 'tp'), may hold values from -270 to 270
- value_cache: bfloat16 [12, 4096, 512], P(None, 'kv', 'tp'), may hold values from -6 to 6
- key_summary: bfloat16 [12, 256, 512], P(None, 'kv', 'tp'), may hold values from -260 to 260
- value_summary: bfloat16 [12, 256, 512], P(None, 'kv', 'tp'), may hold values from -6 to 6
- lengths: int32 [12], replicated, may hold values from 16 to 4096, as said below
- chosen: int32 [12, 4, 128], P(None, 'tp', 'kv'), may hold values from 0 to 1, as said below
Outputs:
- attended: bfloat16 [12, 2048], P(None, 'tp')
Inputs may be any that keep to these rules, and one draw needn't show every extreme that they name: `lengths`: at least one sequence has length 4096. `chosen`: for each sequence s and key head, exactly min(16, live blocks) entries are 1, the live blocks being those that hold a position below lengths[s]; block 0, block 64 when it is live, and the block holding position lengths[s] - 1 are among them, and no block beyond is.
All inputs are finite; a program needn't handle non-finite values.
Results may differ from a plain program's by a relative error of at most 0.012.
Values may be sent and summed in bfloat16 or wider, within the bound.
A program may use at most 64 MiB of HBM per device.

v0:
```python
import jax
import jax.numpy as jnp
from jax import lax
from jax.sharding import PartitionSpec as P

HDIM = 128
SB = 32


neg_fill = -1e30


def joined(value, axis, join):
    pieces = jax.tree.map(lambda part: lax.all_gather(part, axis), value)
    head = jax.tree.map(lambda part: part[0], pieces)
    tail = jax.tree.map(lambda part: part[1:], pieces)
    running, _ = lax.scan(lambda running, section: (join(running, section), None), head, tail)
    return running


def combine_pair(earlier, latter):
    peak_a, total_a, accum_a = earlier
    peak_b, total_b, accum_b = latter
    peak_all = jnp.maximum(peak_a, peak_b)
    factor_a = jnp.exp(peak_a - peak_all)
    factor_b = jnp.exp(peak_b - peak_all)
    return (
        peak_all,
        total_a * factor_a + total_b * factor_b,
        accum_a * factor_a[..., None] + accum_b * factor_b[..., None],
    )


def combine_states(earlier, latter):
    summary_part = combine_pair(earlier[0:3], latter[0:3])
    chosen_part = combine_pair(earlier[3:6], latter[3:6])
    return summary_part + chosen_part


def weigh_rows(scores, live_mask, peak_all, values):
    weights = jnp.where(live_mask, jnp.exp(scores - peak_all[..., None]), 0.0)
    return (jnp.sum(weights, axis=-1), jnp.einsum("sgrn,sngd->sgrd", weights, values))


def local(
    tokens,
    w_query,
    w_key,
    w_value,
    w_gate,
    w_out,
    key_cache,
    value_cache,
    key_summary,
    value_summary,
    lengths,
    chosen,
):
    head_size = HDIM
    group_count = w_key.shape[1] // head_size
    head_count = w_query.shape[1] // head_size
    per_group = head_count // group_count
    seq_count = tokens.shape[0]
    local_rows = key_cache.shape[1]
    summary_rows = key_summary.shape[1]
    stride = local_rows // summary_rows
    score_scale = head_size ** (-0.5)
    queries = jnp.dot(tokens, w_query, preferred_element_type=jnp.float32).astype(jnp.bfloat16)
    new_keys = jnp.dot(tokens, w_key, preferred_element_type=jnp.float32).astype(jnp.bfloat16)
    new_values = jnp.dot(tokens, w_value, preferred_element_type=jnp.float32).astype(jnp.bfloat16)
    head_start = lax.axis_index("tp") * head_count
    gate_cols = lax.dynamic_slice_in_dim(w_gate, 2 * head_start, 2 * head_count, 1)
    gate_vals = jax.nn.sigmoid(jnp.dot(tokens, gate_cols, preferred_element_type=jnp.float32))
    gate_vals = gate_vals.reshape(seq_count, group_count, per_group, 2)
    dev_index = lax.axis_index("kv")
    grouped = queries.reshape(seq_count, group_count, per_group, head_size)
    summary_index = dev_index * summary_rows + jnp.arange(summary_rows)
    live_sum = ((summary_index + 1) * stride <= lengths[:, None])[:, None, None, :]
    position = dev_index * local_rows + jnp.arange(local_rows)
    chosen_rows = jnp.repeat(chosen, SB, axis=2) != 0
    live_sel = ((position[None, :] < lengths[:, None])[:, None, :] & chosen_rows)[:, :, None, :]
    sum_scores = (
        jnp.einsum(
            "sgrd,sngd->sgrn",
            grouped,
            key_summary.reshape(seq_count, summary_rows, group_count, head_size),
            preferred_element_type=jnp.float32,
        )
        * score_scale
    )
    sum_scores = jnp.where(live_sum, sum_scores, neg_fill)
    sel_scores = (
        jnp.einsum(
            "sgrd,sngd->sgrn",
            grouped,
            key_cache.reshape(seq_count, local_rows, group_count, head_size),
            preferred_element_type=jnp.float32,
        )
        * score_scale
    )
    sel_scores = jnp.where(live_sel, sel_scores, neg_fill)
    sum_values = value_summary.reshape(seq_count, summary_rows, group_count, head_size).astype(
        jnp.float32
    )
    sel_values = value_cache.reshape(seq_count, local_rows, group_count, head_size).astype(
        jnp.float32
    )
    sum_peak = jnp.max(sum_scores, axis=-1)
    sel_peak = jnp.max(sel_scores, axis=-1)
    sum_total, sum_accum = weigh_rows(sum_scores, live_sum, sum_peak, sum_values)
    sel_total, sel_accum = weigh_rows(sel_scores, live_sel, sel_peak, sel_values)
    merged = joined(
        (sum_peak, sum_total, sum_accum, sel_peak, sel_total, sel_accum), "kv", combine_states
    )
    sum_peak, sum_total, sum_accum, sel_peak, sel_total, sel_accum = merged
    compressed = sum_accum / sum_total[..., None]
    own_key = new_keys.reshape(seq_count, group_count, 1, head_size).astype(jnp.float32)
    own_value = new_values.reshape(seq_count, group_count, 1, head_size).astype(jnp.float32)
    own_score = jnp.sum(grouped.astype(jnp.float32) * own_key, axis=-1) * score_scale
    peak_all = jnp.maximum(sel_peak, own_score)
    carried = jnp.exp(sel_peak - peak_all)
    own_weight = jnp.exp(own_score - peak_all)
    selected = (sel_accum * carried[..., None] + own_weight[..., None] * own_value) / (
        sel_total * carried + own_weight
    )[..., None]
    mixed_heads = gate_vals[..., 0:1] * compressed + gate_vals[..., 1:2] * selected
    mixed_heads = mixed_heads.reshape(seq_count, head_count * head_size).astype(jnp.bfloat16)
    output = jnp.dot(
        lax.all_gather(mixed_heads, "tp", axis=1, tiled=True),
        w_out,
        preferred_element_type=jnp.float32,
    )
    return output.astype(jnp.bfloat16)


def solution(mesh):
    return jax.shard_map(
        local,
        mesh=mesh,
        in_specs=(
            P(),
            P(None, "tp"),
            P(None, "tp"),
            P(None, "tp"),
            P(),
            P(None, "tp"),
            P(None, "kv", "tp"),
            P(None, "kv", "tp"),
            P(None, "kv", "tp"),
            P(None, "kv", "tp"),
            P(),
            P(None, "tp", "kv"),
        ),
        out_specs=P(None, "tp"),
        check_vma=False,
    )
```

profile of v0, /device:TPU:0, one launch (start us, length us, event | category | flops | bytes accessed | tf_op | source)
XLA Modules:
  0.0 153.5 jit_solution(18045279504071445358)
XLA Ops:
  0.0 0.9 broadcast_compare_fusion.2
  0.9 0.7 broadcast_compare_fusion.1
  1.6 0.1 copy.94
  1.7 0.7 broadcast_compare_fusion
  2.4 1.0 fusion.23
  3.7 1.5 fusion.20
  5.2 1.5 fusion.19
  6.8 0.1 ne.16
  7.0 2.9 %convolution_convert_fusion.1 = bf16[12,1024]{1,0:T(8,128)(2,1)S(1)} fusion(bf16[12,2048]{1,0:T(8,128)(2,1)S(1)} %copy-done.1, bf16[2048,1024]{1,0:T(8,128)(2,1)} %param.15), kind=kOutput, calls=%fused_computation.27 | convolution fusion | flops 50343936 | bytes 4268032 | tf_op jit(solution)/shard_map/dot_general | solution.py:68
  9.9 0.1 multiply_reduce_fusion
  10.1 0.3 fusion.48
  10.4 0.2 fusion.34
  10.6 1.1 fusion.24
  11.7 0.6 fusion.49
  12.3 0.2 fusion.30
  12.6 0.4 fusion.6
  12.9 23.6 %all-gather.3 = f32[192,2,4]{2,1,0:T(2,128)S(1)} all-gather(f32[12,2,4]{2,1,0:T(2,128)S(1)} %get-tuple-element.163), channel_id=5, replica_groups=mesh['kv'=16,'tp'=2] {'kv'}, dimensions={0}, use_global_device_ids=true | all-gather | bytes 6528 | tf_op jit(solution)/shard_map/all_gather | solution.py:14
  36.7 0.3 copy.108
  37.0 18.0 %all-gather.4 = f32[192,2,4]{2,1,0:T(2,128)S(1)} all-gather(f32[12,2,4]{2,1,0:T(2,128)S(1)} %fusion.30), channel_id=6, replica_groups=mesh['kv'=16,'tp'=2] {'kv'}, dimensions={0}, use_global_device_ids=true | all-gather | bytes 6528 | tf_op jit(solution)/shard_map/all_gather | solution.py:14
  55.1 0.3 copy.109
  55.4 19.3 %all-gather = f32[192,2,4]{2,1,0:T(2,128)S(1)} all-gather(f32[12,2,4]{2,1,0:T(2,128)S(1)} %get-tuple-element.161), channel_id=2, replica_groups=mesh['kv'=16,'tp'=2] {'kv'}, dimensions={0}, use_global_device_ids=true | all-gather | bytes 6528 | tf_op jit(solution)/shard_map/all_gather | solution.py:14
  74.8 0.3 copy.106
  75.1 18.0 %all-gather.1 = f32[192,2,4]{2,1,0:T(2,128)S(1)} all-gather(f32[12,2,4]{2,1,0:T(2,128)S(1)} %fusion.34), channel_id=3, replica_groups=mesh['kv'=16,'tp'=2] {'kv'}, dimensions={0}, use_global_device_ids=true | all-gather | bytes 6528 | tf_op jit(solution)/shard_map/all_gather | solution.py:14
  93.1 0.3 copy.107
  93.4 20.9 %all-gather.5 = f32[192,2,4,128]{3,2,1,0:T(4,128)S(1)} all-gather(f32[12,2,4,128]{3,2,1,0:T(4,128)S(1)} %fusion.6), channel_id=7, replica_groups=mesh['kv'=16,'tp'=2] {'kv'}, dimensions={0}, use_global_device_ids=true | all-gather | bytes 835584 | tf_op jit(solution)/shard_map/all_gather | solution.py:14
  114.4 0.1 slice.80
  114.5 19.6 %all-gather.2 = f32[192,2,4,128]{3,2,1,0:T(4,128)S(1)} all-gather(f32[12,2,4,128]{3,2,1,0:T(4,128)S(1)} %fusion.24), channel_id=4, replica_groups=mesh['kv'=16,'tp'=2] {'kv'}, dimensions={0}, use_global_device_ids=true | all-gather | bytes 835584 | tf_op jit(solution)/shard_map/all_gather | solution.py:14
  134.1 0.1 slice.77
  134.2 10.5 %while.20 = (s32[]{:T(128)}, f32[12,2,4]{0,2,1:T(4,128)S(1)}, f32[12,2,4]{0,2,1:T(4,128)S(1)}, f32[12,2,4,128]{3,2,1,0:T(4,128)S(1)}, f32[12,2,4]{0,2,1:T(4,128)...) while((s32[]{:T(128)}, f32[12,2,4]{0,2,1:T(4,128)S(1)}, ...), condition=%wide.region_5.6_spmd, body=%wide.region_4.5_spmd.sunk | while | flops 74882 | bytes 305817 | solution.py:17
  134.7 0.2 fusion.70
  135.4 0.2 fusion.70
  136.1 0.2 fusion.70
  136.8 0.2 fusion.70
  137.5 0.2 fusion.70
  138.2 0.2 fusion.70
  138.9 0.2 fusion.70
  139.6 0.2 fusion.70
  140.3 0.2 fusion.70
  141.0 0.2 fusion.70
  141.7 0.2 fusion.70
  142.4 0.2 fusion.70
  143.1 0.2 fusion.70
  143.8 0.2 fusion.70
  144.5 0.2 fusion.70
  144.8 0.1 copy.116
  145.2 0.2 add_convert_fusion
  145.5 4.6 %all_gather.51 = bf16[12,2048]{1,0:T(8,128)(2,1)S(1)} all-gather(bf16[12,1024]{1,0:T(8,128)(2,1)S(1)} %convert_element_type.54), channel_id=1, replica_groups=mesh['kv'=16,'tp'=2] {'tp'}, dimensions={1}, use_global_device_ids=true | all-gather | bytes 73728 | tf_op jit(solution)/shard_map/all_gather | solution.py:129
  150.0 3.5 %convolution_convert_fusion = bf16[12,1024]{1,0:T(8,128)(2,1)} fusion(bf16[12,2048]{1,0:T(8,128)(2,1)S(1)} %all_gather.51, bf16[2048,1024]{1,0:T(8,128)(2,1)} %param.19), kind=kOutput, calls=%fused_computation.24 | convolution fusion | flops 50343936 | bytes 4268032 | tf_op jit(solution)/shard_map/dot_general | solution.py:128
  (129 shorter events, 8.1 us)
Async XLA Ops:
  0.0 11.7 %copy-start = (bf16[12,256,256]{2,1,0:T(8,128)(2,1)S(1)}, bf16[12,256,256]{2,1,0:T(8,128)(2,1)}, u32[]{:S(2)}) copy-start(bf16[12,256,256]{2,1,0:T(8,128)(2,1)} %param.20) | copy-start | bytes 4718596
  0.0 7.0 %copy-start.1 = (bf16[12,2048]{1,0:T(8,128)(2,1)S(1)}, bf16[12,2048]{1,0:T(8,128)(2,1)}, u32[]{:S(2)}) copy-start(bf16[12,2048]{1,0:T(8,128)(2,1)} %param.14) | copy-start | bytes 147460
  7.0 3.1 %copy-start.3 = (bf16[12,16,256]{2,1,0:T(8,128)(2,1)S(1)}, bf16[12,16,256]{2,1,0:T(8,128)(2,1)}, u32[]{:S(2)}) copy-start(bf16[12,16,256]{2,1,0:T(8,128)(2,1)} %param.22) | copy-start | bytes 294916
  9.9 2.7 %copy-start.2 = (bf16[12,256,256]{2,1,0:T(8,128)(2,1)S(1)}, bf16[12,256,256]{2,1,0:T(8,128)(2,1)}, u32[]{:S(2)}) copy-start(bf16[12,256,256]{2,1,0:T(8,128)(2,1)} %param.21) | copy-start | bytes 4718596
where the time goes:
time: 154 us
  blocking collectives  124 us (81%)
  matrix products  12.7 us (8%)
  local copies, waits for them, and re-layouts  9.02 us (6%)
  other arithmetic  7.29 us (5%)
    all_gather x6, blocking collectives, joined(): pieces = jax.tree.map(lambda part: lax.all_gather(part, axis), value)  119 us
    all_gather x1, blocking collectives, local(): lax.all_gather(mixed_heads, 'tp', axis=1, tiled=True)  4.58 us
    add x15, other arithmetic, combine_pair(): accum_a * factor_a[..., None] + accum_b * factor_b[..., None]  3.47 us
    dot_general x1, matrix products, local(): jnp.dot(lax.all_gather(mixed_heads, 'tp', axis=1, tiled=True), w_out, pre...  3.47 us

commit v1 on v0

v1 whole, which is shorter than its diff:
```python
import functools

import jax
import jax.numpy as jnp
from jax import lax
from jax.experimental import pallas as pl
from jax.experimental.pallas import tpu as pltpu
from jax.sharding import PartitionSpec as P

HDIM = 128
MESH = pl.DeviceIdType.MESH
neg_fill = -1e30
F32 = jnp.float32
BF16 = jnp.bfloat16
NT = (((1,), (1,)), ((), ()))
PIECES = 4


def kernel(
    kv_n, tp_n, heads, groups,
    lengths, tokens, w_query, w_key, w_value, w_gate, w_out, key_cache, value_cache, key_sum, value_sum, chosen,
    out,
    wq, wk, wv, wo, kc, vc, wide_q, scores, picked, new_k, new_v, gates,
    sbuf, rbuf, mine, obuf,
    in_sem, wq_sem, send1, recv1, send2, recv2, loc_sem,
):
    my_kv = lax.axis_index("kv")
    my_tp = lax.axis_index("tp")
    seqs, rows, width = kc.shape
    padded = wide_q.shape[1]
    per_group = heads // groups
    total = seqs * padded
    scale = HDIM ** (-0.5)
    depth = wq.shape[0]
    piece = depth // PIECES

    def query_copy(i):
        part = pl.ds(i * piece, piece)
        return pltpu.make_async_copy(w_query.at[part], wq.at[part], wq_sem.at[i])

    loads = [
        pltpu.make_async_copy(a, b, in_sem.at[i])
        for i, (a, b) in enumerate(
            ((key_cache, kc), (value_cache, vc), (w_key, wk), (w_value, wv), (w_out, wo))
        )
    ]
    for i in range(PIECES):
        query_copy(i).start()
    for load in loads:
        load.start()

    barrier = pltpu.get_barrier_semaphore()

    def each_peer(fn):
        for dt in range(tp_n):
            t = lax.rem(my_tp + dt, tp_n)

            def step(j, carry, t=t):
                fn(lax.rem(my_kv + j, kv_n), t)
                return carry

            lax.fori_loop(1 if dt == 0 else 0, kv_n, step, 0)

    each_peer(lambda k, t: pl.semaphore_signal(barrier, inc=1, device_id=(k, t), device_id_type=MESH))

    row_seq = lax.broadcasted_iota(jnp.int32, (total, 1), 0) // padded
    row_len = jnp.zeros((total, 1), jnp.int32)
    for s in range(seqs):
        row_len = jnp.where(row_seq == s, lengths[s], row_len)
    head_row = lax.broadcasted_iota(jnp.int32, (padded, 1), 0)

    def by_group(parts):
        value = parts[0]
        for g in range(1, groups):
            value = jnp.where(head_row >= g * per_group, parts[g], value)
        return value

    blocks = chosen.shape[2]
    for s in range(seqs):
        flags = chosen[s].astype(F32)
        picked[s] = by_group([jnp.broadcast_to(flags[g : g + 1], (padded, blocks)) for g in range(groups)])
    span = rows // blocks
    spread = (
        lax.broadcasted_iota(jnp.int32, (blocks, rows), 1) // span
        == lax.broadcasted_iota(jnp.int32, (blocks, rows), 0)
    ).astype(F32)
    picked_rows = jnp.dot(picked[...].reshape(total, blocks), spread, preferred_element_type=F32)
    position = my_kv * rows + lax.broadcasted_iota(jnp.int32, (total, rows), 1)
    live_sel = (picked_rows > 0.5) & (position < row_len)
    sum_rows = key_sum.shape[1]
    stride = rows // sum_rows
    col = lax.broadcasted_iota(jnp.int32, (total, seqs * sum_rows), 1)
    entry = my_kv * sum_rows + lax.rem(col, sum_rows)
    live_sum = (col // sum_rows == row_seq) & ((entry + 1) * stride <= row_len)

    queries = jnp.zeros((seqs, wq.shape[1]), F32)
    for i in range(PIECES):
        query_copy(i).wait()
        part = slice(i * piece, (i + 1) * piece)
        queries += jnp.dot(tokens[:, part], wq[part, :], preferred_element_type=F32)
    queries = queries.astype(BF16).astype(F32)
    wide_q[...] = jnp.zeros_like(wide_q)
    for h in range(heads):
        g = h // per_group
        wide_q[:, h, g * HDIM : (g + 1) * HDIM] = queries[:, h * HDIM : (h + 1) * HDIM]

    all_q = wide_q[...].reshape(total, width).astype(BF16)
    ks = key_sum[...].reshape(seqs * sum_rows, width)
    vs = value_sum[...].reshape(seqs * sum_rows, width)

    def soft(raw, live):
        raw = jnp.where(live, raw * scale, neg_fill)
        peak = jnp.max(raw, axis=-1, keepdims=True)
        weights = jnp.where(live, jnp.exp(raw - peak), 0.0)
        return peak, jnp.sum(weights, axis=-1, keepdims=True), weights

    c_peak, c_total, c_weights = soft(lax.dot_general(all_q, ks, NT, preferred_element_type=F32), live_sum)
    c_acc = jnp.dot(c_weights.astype(BF16), vs, preferred_element_type=F32).reshape(seqs, padded, width)

    loads[0].wait()
    for s in range(seqs):
        scores[s] = lax.dot_general(wide_q[s].astype(BF16), kc[s], NT, preferred_element_type=F32)
    s_peak, s_total, s_weights = soft(scores[...].reshape(total, rows), live_sel)
    scores[...] = s_weights.reshape(seqs, padded, rows)
    lane = lax.broadcasted_iota(jnp.int32, (total, HDIM), 1)
    stats = jnp.where(lane == 0, c_peak, jnp.where(lane == 1, c_total, jnp.where(lane == 2, s_peak, s_total)))
    sbuf[:, 2 * padded : 3 * padded, :] = stats.reshape(seqs, padded, HDIM)
    loads[1].wait()
    for s in range(seqs):
        acc = jnp.dot(scores[s].astype(BF16), vc[s], preferred_element_type=F32)
        sbuf[s, 0:padded, :] = by_group([c_acc[s, :, g * HDIM : (g + 1) * HDIM] for g in range(groups)])
        sbuf[s, padded : 2 * padded, :] = by_group([acc[:, g * HDIM : (g + 1) * HDIM] for g in range(groups)])

    pl.semaphore_wait(barrier, kv_n * tp_n - 1)
    owner = my_kv < seqs

    def state_copy(s, slot):
        return pltpu.make_async_remote_copy(
            src_ref=sbuf.at[s], dst_ref=rbuf.at[slot], send_sem=send1.at[s], recv_sem=recv1.at[slot],
            device_id=(s, my_tp), device_id_type=MESH,
        )

    def for_states(fn):
        @pl.when(jnp.logical_not(owner))
        def _():
            fn(lax.rem(my_kv, seqs))

        for j in range(1, seqs):
            fn(lax.rem(my_kv + j, seqs))

    for_states(lambda s: state_copy(s, my_kv).start())

    loads[2].wait()
    loads[3].wait()
    new_k[...] = jnp.dot(tokens[...], wk[...], preferred_element_type=F32).astype(BF16).astype(F32)
    new_v[...] = jnp.dot(tokens[...], wv[...], preferred_element_type=F32).astype(BF16).astype(F32)
    gates[...] = jax.nn.sigmoid(jnp.dot(tokens[...], w_gate[...], preferred_element_type=F32))

    def mixed_copy(k, t):
        return pltpu.make_async_remote_copy(
            src_ref=mine, dst_ref=obuf.at[my_tp, my_kv], send_sem=send2.at[k, t], recv_sem=recv2.at[my_tp, my_kv],
            device_id=(k, t), device_id_type=MESH,
        )

    @pl.when(owner)
    def _():
        rbuf[my_kv] = sbuf[my_kv]

        def got(j, carry):
            slot = lax.rem(my_kv + j, kv_n)
            state_copy(0, slot).wait_recv()
            return carry

        lax.fori_loop(1, kv_n, got, 0)
        chunk = min(kv_n, 16)

        def fold(first, branch):
            tile = rbuf[first : first + chunk, 2 * padded : 3 * padded, :]
            peak = tile[:, :, 2 * branch : 2 * branch + 1]
            weight = tile[:, :, 2 * branch + 1 : 2 * branch + 2]
            acc = rbuf[first : first + chunk, branch * padded : (branch + 1) * padded, :]
            top = jnp.max(peak, axis=0)
            factor = jnp.exp(peak - top[None])
            return top, jnp.sum(weight * factor, axis=0), jnp.sum(acc * factor, axis=0)

        def merge(a, b):
            top = jnp.maximum(a[0], b[0])
            fa, fb = jnp.exp(a[0] - top), jnp.exp(b[0] - top)
            return top, a[1] * fa + b[1] * fb, a[2] * fa + b[2] * fb

        states = []
        for branch in range(2):
            state = fold(0, branch)
            for first in range(chunk, kv_n, chunk):
                state = merge(state, fold(first, branch))
            states.append(state)
        compressed = states[0][2] / states[0][1]
        my_q = wide_q[my_kv]
        my_k = new_k[pl.ds(my_kv, 1), :]
        my_v = new_v[pl.ds(my_kv, 1), :]
        own_score = jnp.sum(my_q * my_k, axis=-1, keepdims=True) * scale
        own_value = by_group(
            [jnp.broadcast_to(my_v[:, g * HDIM : (g + 1) * HDIM], (padded, HDIM)) for g in range(groups)]
        )
        _, weight, acc = merge(states[1], (own_score, jnp.ones_like(own_score), own_value))
        selected = acc / weight
        my_gates = gates[pl.ds(my_kv, 1), :]
        gate_col = lax.broadcasted_iota(jnp.int32, (padded, my_gates.shape[1]), 1)
        first_col = 2 * (my_tp * heads + head_row)

        def gate(branch):
            hit = gate_col == first_col + branch
            return jnp.sum(jnp.where(hit, my_gates, 0.0), axis=-1, keepdims=True)

        mixed = gate(0) * compressed + gate(1) * selected
        mixed = mixed.astype(BF16).astype(F32)
        mine[...] = mixed
        obuf[my_tp, my_kv] = mixed
        each_peer(lambda k, t: mixed_copy(k, t).start())

    loads[4].wait()
    for t in range(tp_n):
        for s in range(seqs):

            @pl.when(jnp.logical_or(my_tp != t, my_kv != s))
            def _():
                pltpu.make_async_remote_copy(
                    src_ref=mine, dst_ref=obuf.at[t, s], send_sem=send2.at[0, 0], recv_sem=recv2.at[t, s],
                    device_id=(my_kv, my_tp), device_id_type=MESH,
                ).wait_recv()

    mixed_all = jnp.concatenate(
        [obuf[t, :, h, :] for t in range(tp_n) for h in range(heads)], axis=1
    ).astype(BF16)
    out[...] = jnp.dot(mixed_all, wo[...], preferred_element_type=F32).astype(BF16)

    for_states(lambda s: state_copy(s, my_kv).wait_send())

    @pl.when(owner)
    def _():
        each_peer(lambda k, t: mixed_copy(k, t).wait_send())


def solution(mesh):
    kv_n, tp_n = mesh.shape["kv"], mesh.shape["tp"]

    def local(
        tokens, w_query, w_key, w_value, w_gate, w_out, key_cache, value_cache, key_sum, value_sum, lengths, chosen
    ):
        seqs, rows, width = key_cache.shape
        heads, groups = w_query.shape[1] // HDIM, w_key.shape[1] // HDIM
        padded = -(-heads // 8) * 8
        assert kv_n >= seqs
        vmem = pl.BlockSpec(memory_space=pltpu.VMEM)
        hbm = pl.BlockSpec(memory_space=pl.ANY)
        smem = pl.BlockSpec(memory_space=pltpu.SMEM)
        dma = pltpu.SemaphoreType.DMA
        return pl.pallas_call(
            functools.partial(kernel, kv_n, tp_n, heads, groups),
            out_shape=jax.ShapeDtypeStruct((seqs, w_out.shape[1]), BF16),
            in_specs=[smem, vmem, hbm, hbm, hbm, vmem, hbm, hbm, hbm, vmem, vmem, vmem],
            out_specs=vmem,
            scratch_shapes=[
                pltpu.VMEM(w_query.shape, BF16),
                pltpu.VMEM(w_key.shape, BF16),
                pltpu.VMEM(w_value.shape, BF16),
                pltpu.VMEM(w_out.shape, BF16),
                pltpu.VMEM(key_cache.shape, BF16),
                pltpu.VMEM(value_cache.shape, BF16),
                pltpu.VMEM((seqs, padded, width), F32),
                pltpu.VMEM((seqs, padded, rows), F32),
                pltpu.VMEM((seqs, padded, chosen.shape[2]), F32),
                pltpu.VMEM((seqs, width), F32),
                pltpu.VMEM((seqs, width), F32),
                pltpu.VMEM((seqs, w_gate.shape[1]), F32),
                pltpu.VMEM((seqs, 3 * padded, HDIM), F32),
                pltpu.VMEM((kv_n, 3 * padded, HDIM), F32),
                pltpu.VMEM((padded, HDIM), F32),
                pltpu.VMEM((tp_n, seqs, padded, HDIM), F32),
                dma((5,)),
                dma((PIECES,)),
                dma((seqs,)),
                dma((kv_n,)),
                dma((kv_n, tp_n)),
                dma((tp_n, seqs)),
                dma((1,)),
            ],
            compiler_params=pltpu.CompilerParams(collective_id=0, has_side_effects=True),
            name="decode",
        )(lengths, tokens, w_query, w_key, w_value, w_gate, w_out, key_cache, value_cache, key_sum, value_sum, chosen)

    return jax.shard_map(
        local,
        mesh=mesh,
        in_specs=(
            P(),
            P(None, "tp"),
            P(None, "tp"),
            P(None, "tp"),
            P(),
            P(None, "tp"),
            P(None, "kv", "tp"),
            P(None, "kv", "tp"),
            P(None, "kv", "tp"),
            P(None, "kv", "tp"),
            P(),
            P(None, "tp", "kv"),
        ),
        out_specs=P(None, "tp"),
        check_vma=False,
    )
```

time: 154 us -> 27.6 us (0.18)
  blocking collectives: 124 us -> 0 us
  Pallas kernels: 0 us -> 22.7 us
  matrix products: 12.7 us -> 0 us
  other arithmetic: 7.29 us -> 0 us
  local copies, waits for them, and re-layouts: 9.02 us -> 4.65 us
    all_gather x7 -> x0, blocking collectives: 124 us -> none  [the longest x6 119 us: joined(): pieces = jax.tree.map(lambda part: lax.all_gather(part, axis), value)]
    pallas_call x0 -> x1, Pallas kernels: none -> 22.7 us  [local(): pl.pallas_call(functools.partial(kernel, kv_n, tp_n, heads, groups), out_...]
    dot_general x9 -> x0, matrix products: 12.7 us -> none  [the longest x1 3.47 us: local(): jnp.dot(lax.all_gather(mixed_heads, 'tp', axis=1, tiled=True), w_out, pre...]
    exp x62 -> x0, local copies, waits for them, and re-layouts: 6.21 us -> none  [the longest x30 3.01 us: combine_pair(): factor_b = jnp.exp(peak_b - peak_all)]
    unnamed x8 -> x3, local copies, waits for them, and re-layouts: 0.02 us -> 4.65 us
    add x47 -> x0, other arithmetic: 4.24 us -> none  [the longest x15 3.47 us: combine_pair(): accum_a * factor_a[..., None] + accum_b * factor_b[..., None]]
    while x9 -> x0, local copies, waits for them, and re-layouts: 1.67 us -> none  [joined(): lax.scan(lambda running, section: (join(running, section), None), head, t...]
where the time goes in v1:
time: 27.6 us; the launch traced here: 27.4 us
  Pallas kernels  22.7 us (82%)
  local copies, waits for them, and re-layouts  4.65 us (17%)
    pallas_call x1, Pallas kernels, local(): pl.pallas_call(functools.partial(kernel, kv_n, tp_n, heads, groups), out_...  22.7 us
    unnamed x3, local copies, waits for them, and re-layouts  4.65 us

profile of v1, /device:TPU:0, one launch (start us, length us, event | category | flops | bytes accessed | tf_op | source)
XLA Modules:
  0.0 27.4 jit_solution(17505968374268051821)
XLA Ops:
  0.0 1.4 %copy.14.chosen = s32[12,2,8]{2,1,0:T(2,128)} copy(s32[12,2,8]{0,2,1:T(8,128)} %param.23) | data formatting | bytes 1536 | tf_op args[11]
  1.4 1.9 %copy.13.w_gate = bf16[2048,32]{1,0:T(8,128)(2,1)} copy(bf16[2048,32]{0,1:T(8,128)(2,1)} %param.16) | data formatting | bytes 262144 | tf_op args[4]
  3.3 22.7 %decode.1 = bf16[12,1024]{1,0:T(8,128)(2,1)} custom-call(s32[12]{0:T(128)} %lengths.1, bf16[12,2048]{1,0:T(8,128)(2,1)} %tokens.1, bf16[2048,1024]{1,0:T(8,128)(2,1)} %w_query.1, bf16[2048,256]{1,0:T(8,128)(2,1)} %w_key.1, bf16[2048,256]{1,0:T(8,128)(2,1)} %w_value.1, bf16[2048,32]{1,0:T(8,128)(2,1)} %copy.13.w_gate, bf16[2048,1024]{1,0:T(8,128)(2,1)} %w_out.1, ...), custom_call_target="tpu_custom_call" | custom-call | tf_op jit(solution)/shard_map/decode/pallas_call | solution.py:258
  26.0 1.4 %copy.16 = bf16[12,1024]{1,0:T(8,128)(2,1)} copy(bf16[12,1024]{1,0:T(8,128)(2,1)} %decode.1) | data formatting | bytes 49152

commit v2 on v1

--- a/solution.py
+++ b/solution.py
@@ -18,11 +18,12 @@
 
 def kernel(
     kv_n, tp_n, heads, groups,
-    lengths, tokens, w_query, w_key, w_value, w_gate, w_out, key_cache, value_cache, key_sum, value_sum, chosen,
+    lengths, tokens_in, w_query, w_key, w_value, w_gate_in, w_out, key_cache, value_cache, key_in, value_in, chosen_in,
     out,
-    wq, wk, wv, wo, kc, vc, wide_q, scores, picked, new_k, new_v, gates,
+    tokens, w_gate, key_sum, value_sum, chosen, heads_f32,
+    wq, wk, wv, wo, kc, vc, wide_q, scores, new_k, new_v, gates,
     sbuf, rbuf, mine, obuf,
-    in_sem, wq_sem, send1, recv1, send2, recv2, loc_sem,
+    in_sem, wq_sem, send1, recv1, send2, recv2,
 ):
     my_kv = lax.axis_index("kv")
     my_tp = lax.axis_index("tp")
@@ -41,13 +42,18 @@
     loads = [
         pltpu.make_async_copy(a, b, in_sem.at[i])
         for i, (a, b) in enumerate(
-            ((key_cache, kc), (value_cache, vc), (w_key, wk), (w_value, wv), (w_out, wo))
+            (
+                (key_cache, kc), (value_cache, vc), (w_key, wk), (w_value, wv), (w_out, wo),
+                (tokens_in, tokens), (chosen_in, chosen), (key_in, key_sum), (value_in, value_sum), (w_gate_in, w_gate),
+            )
         )
     ]
+    loads[5].start()
+    loads[6].start()
     for i in range(PIECES):
         query_copy(i).start()
-    for load in loads:
-        load.start()
+    for i in (7, 8, 0, 1, 2, 3, 9, 4):
+        loads[i].start()
 
     barrier = pltpu.get_barrier_semaphore()
 
@@ -75,16 +81,21 @@
             value = jnp.where(head_row >= g * per_group, parts[g], value)
         return value
 
-    blocks = chosen.shape[2]
-    for s in range(seqs):
-        flags = chosen[s].astype(F32)
-        picked[s] = by_group([jnp.broadcast_to(flags[g : g + 1], (padded, blocks)) for g in range(groups)])
+    blocks = chosen.shape[1]
     span = rows // blocks
     spread = (
         lax.broadcasted_iota(jnp.int32, (blocks, rows), 1) // span
         == lax.broadcasted_iota(jnp.int32, (blocks, rows), 0)
     ).astype(F32)
-    picked_rows = jnp.dot(picked[...].reshape(total, blocks), spread, preferred_element_type=F32)
+    to_row = lax.broadcasted_iota(jnp.int32, (seqs, total), 1)
+    same_seq = to_row // padded == lax.broadcasted_iota(jnp.int32, (seqs, total), 0)
+    row_group = jnp.minimum(lax.rem(to_row, padded) // per_group, groups - 1)
+    loads[6].wait()
+    flags = jnp.zeros((blocks, total), F32)
+    for g in range(groups):
+        place = (same_seq & (row_group == g)).astype(F32)
+        flags += jnp.dot(chosen[g].astype(F32), place, preferred_element_type=F32)
+    picked_rows = lax.dot_general(flags, spread, (((0,), (0,)), ((), ())), preferred_element_type=F32)
     position = my_kv * rows + lax.broadcasted_iota(jnp.int32, (total, rows), 1)
     live_sel = (picked_rows > 0.5) & (position < row_len)
     sum_rows = key_sum.shape[1]
@@ -93,6 +104,7 @@
     entry = my_kv * sum_rows + lax.rem(col, sum_rows)
     live_sum = (col // sum_rows == row_seq) & ((entry + 1) * stride <= row_len)
 
+    loads[5].wait()
     queries = jnp.zeros((seqs, wq.shape[1]), F32)
     for i in range(PIECES):
         query_copy(i).wait()
@@ -105,6 +117,8 @@
         wide_q[:, h, g * HDIM : (g + 1) * HDIM] = queries[:, h * HDIM : (h + 1) * HDIM]
 
     all_q = wide_q[...].reshape(total, width).astype(BF16)
+    loads[7].wait()
+    loads[8].wait()
     ks = key_sum[...].reshape(seqs * sum_rows, width)
     vs = value_sum[...].reshape(seqs * sum_rows, width)
 
@@ -123,48 +137,60 @@
     s_peak, s_total, s_weights = soft(scores[...].reshape(total, rows), live_sel)
     scores[...] = s_weights.reshape(seqs, padded, rows)
     lane = lax.broadcasted_iota(jnp.int32, (total, HDIM), 1)
-    stats = jnp.where(lane == 0, c_peak, jnp.where(lane == 1, c_total, jnp.where(lane == 2, s_peak, s_total)))
-    sbuf[:, 2 * padded : 3 * padded, :] = stats.reshape(seqs, padded, HDIM)
+    which = lax.rem(lane, 4)
+    stats = jnp.where(which == 0, c_peak, jnp.where(which == 1, c_total, jnp.where(which == 2, s_peak, s_total)))
+    high = stats.astype(BF16).astype(F32)
+    rest = stats - high
+    middle = rest.astype(BF16).astype(F32)
+    stats = jnp.where(lane < 4, high, jnp.where(lane < 8, middle, rest - middle)).reshape(seqs, padded, HDIM)
     loads[1].wait()
     for s in range(seqs):
         acc = jnp.dot(scores[s].astype(BF16), vc[s], preferred_element_type=F32)
-        sbuf[s, 0:padded, :] = by_group([c_acc[s, :, g * HDIM : (g + 1) * HDIM] for g in range(groups)])
-        sbuf[s, padded : 2 * padded, :] = by_group([acc[:, g * HDIM : (g + 1) * HDIM] for g in range(groups)])
+        sbuf[s] = jnp.concatenate(
+            [
+                by_group([c_acc[s, :, g * HDIM : (g + 1) * HDIM] for g in range(groups)]),
+                by_group([acc[:, g * HDIM : (g + 1) * HDIM] for g in range(groups)]),
+                stats[s],
+            ],
+            axis=0,
+        ).astype(BF16)
 
     pl.semaphore_wait(barrier, kv_n * tp_n - 1)
-    owner = my_kv < seqs
+    my_seq = lax.div(my_kv * seqs + (kv_n - 1), kv_n)
+    owner = lax.div(my_seq * kv_n, seqs) == my_kv
 
     def state_copy(s, slot):
         return pltpu.make_async_remote_copy(
             src_ref=sbuf.at[s], dst_ref=rbuf.at[slot], send_sem=send1.at[s], recv_sem=recv1.at[slot],
-            device_id=(s, my_tp), device_id_type=MESH,
+            device_id=(lax.div(s * kv_n, seqs), my_tp), device_id_type=MESH,
         )
 
     def for_states(fn):
         @pl.when(jnp.logical_not(owner))
         def _():
-            fn(lax.rem(my_kv, seqs))
+            fn(lax.rem(my_seq, seqs))
 
         for j in range(1, seqs):
-            fn(lax.rem(my_kv + j, seqs))
+            fn(lax.rem(my_seq + j, seqs))
 
     for_states(lambda s: state_copy(s, my_kv).start())
 
     loads[2].wait()
     loads[3].wait()
+    loads[9].wait()
     new_k[...] = jnp.dot(tokens[...], wk[...], preferred_element_type=F32).astype(BF16).astype(F32)
     new_v[...] = jnp.dot(tokens[...], wv[...], preferred_element_type=F32).astype(BF16).astype(F32)
-    gates[...] = jax.nn.sigmoid(jnp.dot(tokens[...], w_gate[...], preferred_element_type=F32))
+    gates[...] = jax.nn.sigmoid(lax.dot_general(tokens[...], w_gate[...], NT, preferred_element_type=F32))
 
     def mixed_copy(k, t):
         return pltpu.make_async_remote_copy(
-            src_ref=mine, dst_ref=obuf.at[my_tp, my_kv], send_sem=send2.at[k, t], recv_sem=recv2.at[my_tp, my_kv],
+            src_ref=mine, dst_ref=obuf.at[my_tp, my_seq], send_sem=send2.at[k, t], recv_sem=recv2.at[my_tp, my_seq],
             device_id=(k, t), device_id_type=MESH,
         )
 
     @pl.when(owner)
     def _():
-        rbuf[my_kv] = sbuf[my_kv]
+        rbuf[my_kv] = sbuf[my_seq]
 
         def got(j, carry):
             slot = lax.rem(my_kv + j, kv_n)
@@ -175,10 +201,12 @@
         chunk = min(kv_n, 16)
 
         def fold(first, branch):
-            tile = rbuf[first : first + chunk, 2 * padded : 3 * padded, :]
+            block = rbuf[first : first + chunk].astype(F32)
+            tile = block[:, 2 * padded : 3 * padded, 0:12]
+            tile = tile[:, :, 0:4] + tile[:, :, 4:8] + tile[:, :, 8:12]
             peak = tile[:, :, 2 * branch : 2 * branch + 1]
             weight = tile[:, :, 2 * branch + 1 : 2 * branch + 2]
-            acc = rbuf[first : first + chunk, branch * padded : (branch + 1) * padded, :]
+            acc = block[:, branch * padded : (branch + 1) * padded, :]
             top = jnp.max(peak, axis=0)
             factor = jnp.exp(peak - top[None])
             return top, jnp.sum(weight * factor, axis=0), jnp.sum(acc * factor, axis=0)
@@ -195,16 +223,16 @@
                 state = merge(state, fold(first, branch))
             states.append(state)
         compressed = states[0][2] / states[0][1]
-        my_q = wide_q[my_kv]
-        my_k = new_k[pl.ds(my_kv, 1), :]
-        my_v = new_v[pl.ds(my_kv, 1), :]
+        my_q = wide_q[my_seq]
+        my_k = new_k[pl.ds(my_seq, 1), :]
+        my_v = new_v[pl.ds(my_seq, 1), :]
         own_score = jnp.sum(my_q * my_k, axis=-1, keepdims=True) * scale
         own_value = by_group(
             [jnp.broadcast_to(my_v[:, g * HDIM : (g + 1) * HDIM], (padded, HDIM)) for g in range(groups)]
         )
         _, weight, acc = merge(states[1], (own_score, jnp.ones_like(own_score), own_value))
         selected = acc / weight
-        my_gates = gates[pl.ds(my_kv, 1), :]
+        my_gates = gates[pl.ds(my_seq, 1), :]
         gate_col = lax.broadcasted_iota(jnp.int32, (padded, my_gates.shape[1]), 1)
         first_col = 2 * (my_tp * heads + head_row)
 
@@ -213,24 +241,25 @@
             return jnp.sum(jnp.where(hit, my_gates, 0.0), axis=-1, keepdims=True)
 
         mixed = gate(0) * compressed + gate(1) * selected
-        mixed = mixed.astype(BF16).astype(F32)
+        mixed = mixed.astype(BF16)
         mine[...] = mixed
-        obuf[my_tp, my_kv] = mixed
+        obuf[my_tp, my_seq] = mixed
         each_peer(lambda k, t: mixed_copy(k, t).start())
 
     loads[4].wait()
     for t in range(tp_n):
         for s in range(seqs):
 
-            @pl.when(jnp.logical_or(my_tp != t, my_kv != s))
+            @pl.when(jnp.logical_or(my_tp != t, my_kv != s * kv_n // seqs))
             def _():
                 pltpu.make_async_remote_copy(
                     src_ref=mine, dst_ref=obuf.at[t, s], send_sem=send2.at[0, 0], recv_sem=recv2.at[t, s],
                     device_id=(my_kv, my_tp), device_id_type=MESH,
                 ).wait_recv()
 
+    heads_f32[...] = obuf[...].astype(F32)
     mixed_all = jnp.concatenate(
-        [obuf[t, :, h, :] for t in range(tp_n) for h in range(heads)], axis=1
+        [heads_f32[t, :, h, :] for t in range(tp_n) for h in range(heads)], axis=1
     ).astype(BF16)
     out[...] = jnp.dot(mixed_all, wo[...], preferred_element_type=F32).astype(BF16)
 
@@ -258,9 +287,15 @@
         return pl.pallas_call(
             functools.partial(kernel, kv_n, tp_n, heads, groups),
             out_shape=jax.ShapeDtypeStruct((seqs, w_out.shape[1]), BF16),
-            in_specs=[smem, vmem, hbm, hbm, hbm, vmem, hbm, hbm, hbm, vmem, vmem, vmem],
+            in_specs=[smem] + [hbm] * 11,
             out_specs=vmem,
             scratch_shapes=[
+                pltpu.VMEM(tokens.shape, BF16),
+                pltpu.VMEM(w_gate.shape[::-1], BF16),
+                pltpu.VMEM(key_sum.shape, BF16),
+                pltpu.VMEM(value_sum.shape, BF16),
+                pltpu.VMEM((groups, chosen.shape[2], seqs), jnp.int32),
+                pltpu.VMEM((tp_n, seqs, padded, HDIM), F32),
                 pltpu.VMEM(w_query.shape, BF16),
                 pltpu.VMEM(w_key.shape, BF16),
                 pltpu.VMEM(w_value.shape, BF16),
@@ -269,25 +304,26 @@
                 pltpu.VMEM(value_cache.shape, BF16),
                 pltpu.VMEM((seqs, padded, width), F32),
                 pltpu.VMEM((seqs, padded, rows), F32),
-                pltpu.VMEM((seqs, padded, chosen.shape[2]), F32),
                 pltpu.VMEM((seqs, width), F32),
                 pltpu.VMEM((seqs, width), F32),
                 pltpu.VMEM((seqs, w_gate.shape[1]), F32),
-                pltpu.VMEM((seqs, 3 * padded, HDIM), F32),
-                pltpu.VMEM((kv_n, 3 * padded, HDIM), F32),
-                pltpu.VMEM((padded, HDIM), F32),
-                pltpu.VMEM((tp_n, seqs, padded, HDIM), F32),
-                dma((5,)),
+                pltpu.VMEM((seqs, 3 * padded, HDIM), BF16),
+                pltpu.VMEM((kv_n, 3 * padded, HDIM), BF16),
+                pltpu.VMEM((padded, HDIM), BF16),
+                pltpu.VMEM((tp_n, seqs, padded, HDIM), BF16),
+                dma((10,)),
                 dma((PIECES,)),
                 dma((seqs,)),
                 dma((kv_n,)),
                 dma((kv_n, tp_n)),
                 dma((tp_n, seqs)),
-                dma((1,)),
             ],
             compiler_params=pltpu.CompilerParams(collective_id=0, has_side_effects=True),
             name="decode",
-        )(lengths, tokens, w_query, w_key, w_value, w_gate, w_out, key_cache, value_cache, key_sum, value_sum, chosen)
+        )(
+            lengths, tokens, w_query, w_key, w_value, w_gate.T, w_out, key_cache, value_cache, key_sum, value_sum,
+            jnp.transpose(chosen, (1, 2, 0)),
+        )
 
     return jax.shard_map(
         local,

time: 27.6 us -> 22.3 us (0.81)
  local copies, waits for them, and re-layouts: 4.65 us -> 1.38 us
  Pallas kernels: 22.7 us -> 20.8 us
    unnamed x3 -> x1, local copies, waits for them, and re-layouts: 4.65 us -> 1.38 us
    pallas_call x1, Pallas kernels: 22.7 us -> 20.8 us  [local(): pl.pallas_call(functools.partial(kernel, kv_n, tp_n, heads, groups), out_...]
where the time goes in v2:
time: 22.3 us; the launch traced here: 22.2 us
  Pallas kernels  20.8 us (93%)
  local copies, waits for them, and re-layouts  1.38 us (6%)
    pallas_call x1, Pallas kernels, local(): pl.pallas_call(functools.partial(kernel, kv_n, tp_n, heads, groups), out_...  20.8 us
    unnamed x1, local copies, waits for them, and re-layouts  1.38 us

profile of v2, /device:TPU:0, one launch (start us, length us, event | category | flops | bytes accessed | tf_op | source)
XLA Modules:
  0.0 22.2 jit_solution(10300766096496169421)
XLA Ops:
  0.0 20.8 %decode.1 = bf16[12,1024]{1,0:T(8,128)(2,1)} custom-call(s32[12]{0:T(128)} %lengths.1, bf16[12,2048]{1,0:T(8,128)(2,1)} %tokens_in.1, bf16[2048,1024]{1,0:T(8,128)(2,1)} %w_query.1, bf16[2048,256]{1,0:T(8,128)(2,1)} %w_key.1, bf16[2048,256]{1,0:T(8,128)(2,1)} %w_value.1, bf16[32,2048]{1,0:T(8,128)(2,1)} %bitcast.2, bf16[2048,1024]{1,0:T(8,128)(2,1)} %w_out.1, ...), custom_call_target="tpu_custom_call" | custom-call | tf_op jit(solution)/shard_map/decode/pallas_call | solution.py:287
  20.8 1.4 %copy.14 = bf16[12,1024]{1,0:T(8,128)(2,1)} copy(bf16[12,1024]{1,0:T(8,128)(2,1)} %decode.1) | data formatting | bytes 49152

commit v3 on v2

--- a/solution.py
+++ b/solution.py
@@ -57,7 +57,7 @@
 
     barrier = pltpu.get_barrier_semaphore()
 
-    def each_peer(fn):
+    def each_peer(fn, straight=kv_n <= 16):
         for dt in range(tp_n):
             t = lax.rem(my_tp + dt, tp_n)
 
@@ -65,7 +65,12 @@
                 fn(lax.rem(my_kv + j, kv_n), t)
                 return carry
 
-            lax.fori_loop(1 if dt == 0 else 0, kv_n, step, 0)
+            first = 1 if dt == 0 else 0
+            if straight:
+                for j in range(first, kv_n):
+                    step(j, 0)
+            else:
+                lax.fori_loop(first, kv_n, step, 0)
 
     each_peer(lambda k, t: pl.semaphore_signal(barrier, inc=1, device_id=(k, t), device_id_type=MESH))
 
@@ -192,6 +197,23 @@
     def _():
         rbuf[my_kv] = sbuf[my_seq]
 
+        my_q = wide_q[my_seq]
+        my_k = new_k[pl.ds(my_seq, 1), :]
+        my_v = new_v[pl.ds(my_seq, 1), :]
+        own_score = jnp.sum(my_q * my_k, axis=-1, keepdims=True) * scale
+        own_value = by_group(
+            [jnp.broadcast_to(my_v[:, g * HDIM : (g + 1) * HDIM], (padded, HDIM)) for g in range(groups)]
+        )
+        my_gates = gates[pl.ds(my_seq, 1), :]
+        gate_col = lax.broadcasted_iota(jnp.int32, (padded, my_gates.shape[1]), 1)
+        first_col = 2 * (my_tp * heads + head_row)
+
+        def gate(branch):
+            hit = gate_col == first_col + branch
+            return jnp.sum(jnp.where(hit, my_gates, 0.0), axis=-1, keepdims=True)
+
+        gate_c, gate_s = gate(0), gate(1)
+
         def got(j, carry):
             slot = lax.rem(my_kv + j, kv_n)
             state_copy(0, slot).wait_recv()
@@ -223,28 +245,19 @@
                 state = merge(state, fold(first, branch))
             states.append(state)
         compressed = states[0][2] / states[0][1]
-        my_q = wide_q[my_seq]
-        my_k = new_k[pl.ds(my_seq, 1), :]
-        my_v = new_v[pl.ds(my_seq, 1), :]
-        own_score = jnp.sum(my_q * my_k, axis=-1, keepdims=True) * scale
-        own_value = by_group(
-            [jnp.broadcast_to(my_v[:, g * HDIM : (g + 1) * HDIM], (padded, HDIM)) for g in range(groups)]
-        )
         _, weight, acc = merge(states[1], (own_score, jnp.ones_like(own_score), own_value))
         selected = acc / weight
-        my_gates = gates[pl.ds(my_seq, 1), :]
-        gate_col = lax.broadcasted_iota(jnp.int32, (padded, my_gates.shape[1]), 1)
-        first_col = 2 * (my_tp * heads + head_row)
-
-        def gate(branch):
-            hit = gate_col == first_col + branch
-            return jnp.sum(jnp.where(hit, my_gates, 0.0), axis=-1, keepdims=True)
-
-        mixed = gate(0) * compressed + gate(1) * selected
+        mixed = gate_c * compressed + gate_s * selected
         mixed = mixed.astype(BF16)
         mine[...] = mixed
         obuf[my_tp, my_seq] = mixed
         each_peer(lambda k, t: mixed_copy(k, t).start())
+
+    for_states(lambda s: state_copy(s, my_kv).wait_send())
+
+    @pl.when(owner)
+    def _():
+        each_peer(lambda k, t: mixed_copy(k, t).wait_send(), False)
 
     loads[4].wait()
     for t in range(tp_n):
@@ -262,12 +275,6 @@
         [heads_f32[t, :, h, :] for t in range(tp_n) for h in range(heads)], axis=1
     ).astype(BF16)
     out[...] = jnp.dot(mixed_all, wo[...], preferred_element_type=F32).astype(BF16)
-
-    for_states(lambda s: state_copy(s, my_kv).wait_send())
-
-    @pl.when(owner)
-    def _():
-        each_peer(lambda k, t: mixed_copy(k, t).wait_send())
 
 
 def solution(mesh):

time: 22.3 us -> 22 us (0.987)
  Pallas kernels: 20.8 us -> 20.4 us
    pallas_call x1, Pallas kernels: 20.8 us -> 20.4 us  [local(): pl.pallas_call(functools.partial(kernel, kv_n, tp_n, heads, groups), out_...]
where the time goes in v3:
time: 22 us; the launch traced here: 21.8 us
  Pallas kernels  20.4 us (93%)
  local copies, waits for them, and re-layouts  1.38 us (6%)
    pallas_call x1, Pallas kernels, local(): pl.pallas_call(functools.partial(kernel, kv_n, tp_n, heads, groups), out_...  20.4 us
    unnamed x1, local copies, waits for them, and re-layouts  1.38 us

profile of v3, /device:TPU:0, one launch (start us, length us, event | category | flops | bytes accessed | tf_op | source)
XLA Modules:
  0.0 21.8 jit_solution(17316313158957096008)
XLA Ops:
  0.0 20.4 %decode.1 = bf16[12,1024]{1,0:T(8,128)(2,1)} custom-call(s32[12]{0:T(128)} %lengths.1, bf16[12,2048]{1,0:T(8,128)(2,1)} %tokens_in.1, bf16[2048,1024]{1,0:T(8,128)(2,1)} %w_query.1, bf16[2048,256]{1,0:T(8,128)(2,1)} %w_key.1, bf16[2048,256]{1,0:T(8,128)(2,1)} %w_value.1, bf16[32,2048]{1,0:T(8,128)(2,1)} %bitcast.2, bf16[2048,1024]{1,0:T(8,128)(2,1)} %w_out.1, ...), custom_call_target="tpu_custom_call" | custom-call | tf_op jit(solution)/shard_map/decode/pallas_call | solution.py:294
  20.4 1.4 %copy.14 = bf16[12,1024]{1,0:T(8,128)(2,1)} copy(bf16[12,1024]{1,0:T(8,128)(2,1)} %decode.1) | data formatting | bytes 49152
